TPU v7x, 32 devices: a whole 2x2x4 slice. The times are simulated.
32 devices in a mesh: kv: 8 (over z, x), tp: 4 (over y, core).
Axes of the slice: x: 2, y: 2, z: 4, core: 2. Of those that a mesh axis runs over, the one named last changes fastest.
Arguments:
- tokens: bfloat16 [4, 4096], P(None, 'kv'), may hold values from -30 to 30
- norm_gain: float32 [4096], P('kv'), may hold values from 0.1 to 1.9
- query_weight: bfloat16 [4096, 2048], P('kv', 'tp'), may hold values from -0.09375 to 0.09375
- cache_keys: bfloat16 [4, 4096, 16, 128], P(None, 'kv', 'tp'), may hold values from -180 to 180
- cache_values: bfloat16 [4, 4096, 16, 128], P(None, 'kv', 'tp'), may hold values from -6 to 6
- lengths: int32 [4], replicated, may hold values from 2049 to 4096, as said below
- lambdas: float32 [16], P('tp'), may hold values from 0.3 to 0.8
- head_gain: float32 [128], replicated, may hold values from 0.1 to 1.9
- out_weight: bfloat16 [2048, 4096], P('tp', 'kv'), may hold values from -0.125 to 0.125
Outputs:
- mixed: bfloat16 [4, 4096], P(None, 'kv')
Inputs may be any that keep to these rules, and one draw needn't show every extreme that they name: `lengths`: every length is more than half of 4096; some sequence has exactly 4096.
All inputs are finite; a program needn't handle non-finite values.
Results may differ from a plain program's by a relative error of at most 0.02.
Values may be sent and summed in bfloat16 or wider, within the bound.
No kernel may reach another device: no remote copies, remote signals or barrier semaphores. Data moves between devices by JAX's collectives and lax.ppermute only.
A program may use at most 64 MiB of HBM per device.

v0:
```python
import jax
import jax.numpy as jnp
from jax import lax
from jax.sharding import PartitionSpec as P

D = 4096
HD = 64
VD = 128
eps = 1e-06
NEG = -1e30


def body(
    tokens,
    norm_gain,
    query_weight,
    cache_keys,
    cache_values,
    lengths,
    lambdas,
    head_gain,
    out_weight,
):
    seqs = tokens.shape[0]
    span = cache_keys.shape[1]
    local_heads = cache_keys.shape[2]
    floats = tokens.astype(jnp.float32)
    squares = jnp.sum(floats * floats, axis=1)
    scaled_logits = (floats * norm_gain).astype(jnp.bfloat16)
    partial_value = jnp.dot(scaled_logits, query_weight, preferred_element_type=jnp.float32)
    total_squares, projected = lax.psum((squares, partial_value), "kv")
    inverse = lax.rsqrt(total_squares / D + eps)
    query = (
        (projected * inverse[:, None] * 0.125)
        .astype(jnp.bfloat16)
        .reshape(seqs, local_heads, 2, HD)
    )
    keys = cache_keys.reshape(seqs, span, local_heads, 2, HD)
    score_matrix = jnp.einsum("bhmd,bphmd->bhmp", query, keys, preferred_element_type=jnp.float32)
    position_indices = lax.axis_index("kv") * span + jnp.arange(span, dtype=jnp.int32)
    valid = (position_indices[None, :] < lengths[:, None])[:, None, None, :]
    score_matrix = jnp.where(valid, score_matrix, NEG)
    peak = jnp.max(score_matrix, axis=-1)
    weights = jnp.where(valid, jnp.exp(score_matrix - peak[..., None]), 0.0)
    mass = jnp.sum(weights, axis=-1)
    summed = jnp.einsum(
        "bhmp,bphv->bhmv",
        weights.astype(jnp.bfloat16),
        cache_values,
        preferred_element_type=jnp.float32,
    )
    scales = lambdas[None, :, None]
    whole_peak = lax.pmax(peak, "kv")
    factor = jnp.exp(peak - whole_peak)
    whole_mass = lax.psum(mass * factor, "kv")
    shares = factor / whole_mass
    local_part = (
        summed[:, :, 0] * shares[:, :, 0, None] - scales * summed[:, :, 1] * shares[:, :, 1, None]
    )
    attended = lax.psum(local_part, "kv")
    normed = (
        attended
        * lax.rsqrt(jnp.mean(attended * attended, axis=-1, keepdims=True) + eps)
        * head_gain
        * 0.8
    )
    normed = normed.astype(jnp.bfloat16).reshape(seqs, local_heads * VD)
    part = jnp.dot(normed, out_weight, preferred_element_type=jnp.float32).astype(jnp.bfloat16)
    return lax.psum(part, "tp").astype(jnp.float32).astype(jnp.bfloat16)


def solution(mesh):
    in_specs = (
        P(None, "kv"),
        P("kv"),
        P("kv", "tp"),
        P(None, "kv", "tp", None),
        P(None, "kv", "tp", None),
        P(),
        P("tp"),
        P(),
        P("tp", "kv"),
    )
    out_specs = P(None, "kv")
    return jax.shard_map(body, mesh=mesh, in_specs=in_specs, out_specs=out_specs, check_vma=False)
```

profile of v0, /device:TPU:0, one launch (start us, length us, event | category | flops | bytes accessed | tf_op | source)
XLA Modules:
  0.0 94.3 jit_solution(17817469448406255703)
XLA Ops:
  0.0 0.0 copy-start
  0.0 1.4 %fusion.7 = f32[4,512]{1,0:T(4,128)S(1)} fusion(bf16[512,512]{1,0:T(8,128)(2,1)} %param.11, bf16[4,512]{1,0:T(4,128)(2,1)} %param.9, f32[512]{0:T(512)} %param.10), kind=kOutput, calls=%fused_computation.19 | convolution fusion | flops 2103296 | bytes 538624 | tf_op jit(solution)/shard_map/dot_general | solution.py:30
  1.4 0.8 fusion.5
  2.2 23.6 %all-reduce = (f32[4,512]{1,0:T(4,128)S(1)}, f32[4]{0:T(128)S(1)}) all-reduce(f32[4,512]{1,0:T(4,128)S(1)} %fusion.7, f32[4]{0:T(128)S(1)} %fusion.5), channel_id=1, replica_groups=mesh['kv'=8,'tp'=4] {'kv'}, use_global_device_ids=true, to_apply=%region_0.0 | all-reduce | flops 2052 | bytes 16416 | tf_op jit(solution)/shard_map/psum | solution.py:31
  25.8 0.1 multiply_convert_fusion.1
  25.9 0.1 reshape.55
  26.0 4.3 %copy.20 = bf16[4,512,4,128]{1,3,2,0:T(8,128)(2,1)} copy(bf16[4,512,4,128]{3,2,1,0:T(4,128)(2,1)} %param.12) | data formatting | bytes 4194304 | tf_op args[3]
  30.3 0.0 copy-start.3
  30.3 0.0 copy-start.2
  30.3 0.0 copy-start.4
  30.3 0.0 copy-start.1
  30.3 2.0 %fusion.16 = f32[4,4,2,1,512]{4,3,2,1,0:T(1,128)S(1)} fusion(bf16[4,4,2,64,1]{3,4,2,1,0:T(2,128)(2,1)S(1)} %reshape.55, bf16[4,512,4,2,64]{1,4,3,2,0:T(8,128)(2,1)} %bitcast.33), kind=kOutput, calls=%fused_computation.31 | convolution fusion | flops 2097152 | bytes 2166784 | tf_op jit(solution)/shard_map/bhmd,bphmd->bhmp/dot_general | solution.py:39
  32.3 0.0 copy-done.3
  32.3 0.1 broadcast_compare_fusion
  32.4 0.1 fusion.2
  32.5 0.2 fusion.14
  32.7 17.4 %pmax.7 = f32[4,4,2]{2,1,0:T(4,128)S(1)} all-reduce(f32[4,4,2]{2,1,0:T(4,128)S(1)} %fusion.2), channel_id=1, replica_groups=mesh['kv'=8,'tp'=4] {'kv'}, use_global_device_ids=true, to_apply=%region_4.5 | all-reduce | flops 32 | bytes 256 | tf_op jit(solution)/shard_map/pmax | solution.py:53
  50.1 19.4 %psum.37 = f32[4,4,2]{2,1,0:T(4,128)S(1)} all-reduce(f32[4,4,2]{2,1,0:T(4,128)S(1)} %bitcast.42), channel_id=1, replica_groups=mesh['kv'=8,'tp'=4] {'kv'}, use_global_device_ids=true, to_apply=%region_6.7 | all-reduce | flops 32 | bytes 256 | tf_op jit(solution)/shard_map/psum | solution.py:55
  69.6 0.1 slice_reduce_fusion.1
  69.7 0.0 copy-done
  69.7 0.5 fusion
  70.2 0.0 copy-done.2
  70.2 0.1 multiply_subtract_fusion
  70.3 17.4 %psum.38 = f32[4,4,128]{2,1,0:T(4,128)S(1)} all-reduce(f32[4,4,128]{2,1,0:T(4,128)S(1)} %multiply_subtract_fusion), channel_id=1, replica_groups=mesh['kv'=8,'tp'=4] {'kv'}, use_global_device_ids=true, to_apply=%region_7.8 | all-reduce | flops 2048 | bytes 16384 | tf_op jit(solution)/shard_map/psum | solution.py:60
  87.7 0.1 multiply_reduce_fusion
  87.8 0.0 copy-done.4
  87.8 0.1 fusion.6
  87.8 0.0 copy-done.1
  87.9 0.2 convolution_convert_fusion
  88.0 6.2 %psum.39 = bf16[4,512]{1,0:T(4,128)(2,1)} all-reduce(bf16[4,512]{1,0:T(4,128)(2,1)S(1)} %convolution_convert_fusion), channel_id=1, replica_groups=mesh['kv'=8,'tp'=4] {'tp'}, use_global_device_ids=true, to_apply=%region_9.10 | all-reduce | flops 2048 | bytes 8192 | tf_op jit(solution)/shard_map/psum | solution.py:69
  (6 shorter events, 0.1 us)
Async XLA Ops:
  0.0 69.7 %copy-start = (bf16[4,512,4,128]{3,2,1,0:T(4,128)(2,1)S(1)}, bf16[4,512,4,128]{3,2,1,0:T(4,128)(2,1)}, u32[]{:S(2)}) copy-start(bf16[4,512,4,128]{3,2,1,0:T(4,128)(2,1)} %param.13) | copy-start | bytes 6291460
  30.3 2.0 %copy-start.3 = (s32[4]{0:T(128)S(1)}, s32[4]{0:T(128)}, u32[]{:S(2)}) copy-start(s32[4]{0:T(128)} %param.14) | copy-start | bytes 52
  30.3 39.9 %copy-start.2 = (f32[4]{0:T(128)S(1)}, f32[4]{0:T(128)}, u32[]{:S(2)}) copy-start(f32[4]{0:T(128)} %param.15) | copy-start | bytes 52
  30.3 57.5 %copy-start.4 = (f32[128]{0:T(128)S(1)}, f32[128]{0:T(128)}, u32[]{:S(2)}) copy-start(f32[128]{0:T(128)} %param.16) | copy-start | bytes 1540
  30.3 57.6 %copy-start.1 = (bf16[512,512]{1,0:T(8,128)(2,1)S(1)}, bf16[512,512]{1,0:T(8,128)(2,1)}, u32[]{:S(2)}) copy-start(bf16[512,512]{1,0:T(8,128)(2,1)} %param.17) | copy-start | bytes 1572868
where the time goes:
time: 94.6 us; the launch traced here: 94.3 us
  blocking collectives  84 us (89%)
  local copies, waits for them, and re-layouts  4.54 us (5%)
  matrix products  4.05 us (4%)
  other arithmetic  1.59 us (2%)
    psum x1, blocking collectives, body(): total_squares, projected = lax.psum((squares, partial_value), 'kv')  23.6 us
    psum x1, blocking collectives, body(): whole_mass = lax.psum(mass * factor, 'kv')  19.4 us
    pmax x1, blocking collectives, body(): whole_peak = lax.pmax(peak, 'kv')  17.4 us
    psum x1, blocking collectives, body(): attended = lax.psum(local_part, 'kv')  17.4 us
    psum x1, blocking collectives, body(): return lax.psum(part, 'tp').astype(jnp.float32).astype(jnp.bfloat16)  6.24 us
    unnamed x11, local copies, waits for them, and re-layouts  4.29 us
    dot_general x1, matrix products, body(): jnp.einsum('bhmd,bphmd->bhmp', query, keys, preferred_element_type=jnp.fl...  2.03 us

commit v1 on v0

--- a/solution.py
+++ b/solution.py
@@ -52,7 +52,9 @@
     scales = lambdas[None, :, None]
     whole_peak = lax.pmax(peak, "kv")
     factor = jnp.exp(peak - whole_peak)
-    whole_mass = lax.psum(mass * factor, "kv")
+    x = mass * factor
+    blocks = lax.all_gather(x, "kv")
+    whole_mass = jnp.sum(blocks, axis=0)
     shares = factor / whole_mass
     local_part = (
         summed[:, :, 0] * shares[:, :, 0, None] - scales * summed[:, :, 1] * shares[:, :, 1, None]

time: 94.6 us -> 108 us (1.14)
  blocking collectives: 84 us -> 97.2 us
    all_gather x0 -> x1, blocking collectives: none -> 30.6 us  [body(): blocks = lax.all_gather(x, 'kv')]
    psum x1 -> x0, blocking collectives: 19.4 us -> none  [body(): whole_mass = lax.psum(mass * factor, 'kv')]
    psum x1, blocking collectives: 17.4 us -> 19.4 us  [body(): attended = lax.psum(local_part, 'kv')]
where the time goes in v1:
time: 108 us
  blocking collectives  97.2 us (90%)
  local copies, waits for them, and re-layouts  4.76 us (4%)
  matrix products  4.05 us (4%)
  other arithmetic  1.62 us (2%)
    all_gather x1, blocking collectives, body(): blocks = lax.all_gather(x, 'kv')  30.6 us
    psum x1, blocking collectives, body(): total_squares, projected = lax.psum((squares, partial_value), 'kv')  23.6 us
    psum x1, blocking collectives, body(): attended = lax.psum(local_part, 'kv')  19.4 us
    pmax x1, blocking collectives, body(): whole_peak = lax.pmax(peak, 'kv')  17.4 us
    psum x1, blocking collectives, body(): return lax.psum(part, 'tp').astype(jnp.float32).astype(jnp.bfloat16)  6.24 us
    unnamed x11, local copies, waits for them, and re-layouts  4.29 us

profile of v1, /device:TPU:0, one launch (start us, length us, event | category | flops | bytes accessed | tf_op | source)
XLA Modules:
  0.0 107.7 jit_solution(17429866928546366466)
XLA Ops:
  0.0 0.0 copy-start
  0.0 1.4 %fusion.7 = f32[4,512]{1,0:T(4,128)S(1)} fusion(bf16[512,512]{1,0:T(8,128)(2,1)} %param.11, bf16[4,512]{1,0:T(4,128)(2,1)} %param.9, f32[512]{0:T(512)} %param.10), kind=kOutput, calls=%fused_computation.19 | convolution fusion | flops 2103296 | bytes 538624 | tf_op jit(solution)/shard_map/dot_general | solution.py:30
  1.4 0.8 fusion.5
  2.2 23.6 %all-reduce = (f32[4,512]{1,0:T(4,128)S(1)}, f32[4]{0:T(128)S(1)}) all-reduce(f32[4,512]{1,0:T(4,128)S(1)} %fusion.7, f32[4]{0:T(128)S(1)} %fusion.5), channel_id=1, replica_groups=mesh['kv'=8,'tp'=4] {'kv'}, use_global_device_ids=true, to_apply=%region_0.0 | all-reduce | flops 2052 | bytes 16416 | tf_op jit(solution)/shard_map/psum | solution.py:31
  25.8 0.1 multiply_convert_fusion.1
  25.9 0.1 reshape.56
  26.0 4.3 %copy.25 = bf16[4,512,4,128]{1,3,2,0:T(8,128)(2,1)} copy(bf16[4,512,4,128]{3,2,1,0:T(4,128)(2,1)} %param.12) | data formatting | bytes 4194304 | tf_op args[3]
  30.3 0.0 copy-start.3
  30.3 0.0 copy-start.2
  30.3 0.0 copy-start.4
  30.3 0.0 copy-start.1
  30.3 2.0 %fusion.16 = f32[4,4,2,1,512]{4,3,2,1,0:T(1,128)S(1)} fusion(bf16[4,4,2,64,1]{3,4,2,1,0:T(2,128)(2,1)S(1)} %reshape.56, bf16[4,512,4,2,64]{1,4,3,2,0:T(8,128)(2,1)} %bitcast.34), kind=kOutput, calls=%fused_computation.31 | convolution fusion | flops 2097152 | bytes 2166784 | tf_op jit(solution)/shard_map/bhmd,bphmd->bhmp/dot_general | solution.py:39
  32.3 0.0 copy-done.3
  32.3 0.1 broadcast_compare_fusion
  32.4 0.1 fusion.2
  32.5 0.2 fusion.14
  32.7 17.4 %pmax.7 = f32[4,4,2]{2,1,0:T(4,128)S(1)} all-reduce(f32[4,4,2]{2,1,0:T(4,128)S(1)} %fusion.2), channel_id=1, replica_groups=mesh['kv'=8,'tp'=4] {'kv'}, use_global_device_ids=true, to_apply=%region_4.5 | all-reduce | flops 32 | bytes 256 | tf_op jit(solution)/shard_map/pmax | solution.py:53
  50.1 0.1 copy.28
  50.3 30.6 %all-gather = f32[32,4,2]{1,2,0:T(2,128)S(1)} all-gather(f32[4,4,2]{1,2,0:T(2,128)S(1)} %copy.28), channel_id=2, replica_groups=mesh['kv'=8,'tp'=4] {'kv'}, dimensions={0}, use_global_device_ids=true | all-gather | bytes 1152 | tf_op jit(solution)/shard_map/all_gather | solution.py:56
  80.9 0.1 copy.29
  81.0 0.1 slice_reduce_fusion.1
  81.2 0.0 copy-done
  81.2 0.5 fusion
  81.7 0.0 copy-done.2
  81.7 0.1 multiply_subtract_fusion
  81.7 19.4 %psum.30 = f32[4,4,128]{2,1,0:T(4,128)S(1)} all-reduce(f32[4,4,128]{2,1,0:T(4,128)S(1)} %multiply_subtract_fusion), channel_id=1, replica_groups=mesh['kv'=8,'tp'=4] {'kv'}, use_global_device_ids=true, to_apply=%region_7.8 | all-reduce | flops 2048 | bytes 16384 | tf_op jit(solution)/shard_map/psum | solution.py:62
  101.1 0.1 multiply_reduce_fusion
  101.2 0.0 copy-done.4
  101.2 0.1 fusion.6
  101.3 0.0 copy-done.1
  101.3 0.2 convolution_convert_fusion
  101.5 6.2 %psum.31 = bf16[4,512]{1,0:T(4,128)(2,1)} all-reduce(bf16[4,512]{1,0:T(4,128)(2,1)S(1)} %convolution_convert_fusion), channel_id=1, replica_groups=mesh['kv'=8,'tp'=4] {'tp'}, use_global_device_ids=true, to_apply=%region_9.10 | all-reduce | flops 2048 | bytes 8192 | tf_op jit(solution)/shard_map/psum | solution.py:71
  (7 shorter events, 0.1 us)
Async XLA Ops:
  0.0 81.2 %copy-start = (bf16[4,512,4,128]{3,2,1,0:T(4,128)(2,1)S(1)}, bf16[4,512,4,128]{3,2,1,0:T(4,128)(2,1)}, u32[]{:S(2)}) copy-start(bf16[4,512,4,128]{3,2,1,0:T(4,128)(2,1)} %param.13) | copy-start | bytes 6291460
  30.3 2.0 %copy-start.3 = (s32[4]{0:T(128)S(1)}, s32[4]{0:T(128)}, u32[]{:S(2)}) copy-start(s32[4]{0:T(128)} %param.14) | copy-start | bytes 52
  30.3 51.4 %copy-start.2 = (f32[4]{0:T(128)S(1)}, f32[4]{0:T(128)}, u32[]{:S(2)}) copy-start(f32[4]{0:T(128)} %param.15) | copy-start | bytes 52
  30.3 71.0 %copy-start.4 = (f32[128]{0:T(128)S(1)}, f32[128]{0:T(128)}, u32[]{:S(2)}) copy-start(f32[128]{0:T(128)} %param.16) | copy-start | bytes 1540
  30.3 71.0 %copy-start.1 = (bf16[512,512]{1,0:T(8,128)(2,1)S(1)}, bf16[512,512]{1,0:T(8,128)(2,1)}, u32[]{:S(2)}) copy-start(bf16[512,512]{1,0:T(8,128)(2,1)} %param.17) | copy-start | bytes 1572868
